TPU v7x, 32 devices: a whole 2x2x4 slice. The times are simulated.
32 devices in a mesh: sp: 16 (over z, y, core), tp: 2 (over x).
Axes of the slice: x: 2, y: 2, z: 4, core: 2. Of those that a mesh axis runs over, the one named last changes fastest.
Arguments:
- residual: bfloat16 [2048, 2048], P('sp', 'tp'), may hold values from -24 to 24
- queries: bfloat16 [2048, 2048], P('sp', 'tp'), may hold values from -16 to 16
- key_proj: bfloat16 [2048, 512], P(('sp', 'tp')), may hold values from -8 to 8
- value_proj: bfloat16 [2048, 512], P(('sp', 'tp')), may hold values from -6 to 6
- diff_lambda: float32 [8], replicated, may hold values from 0.3 to 0.8
- head_gain: float32 [256], replicated, may hold values from 0.1 to 1.9
- out_weight: bfloat16 [2048, 2048], P(None, 'tp'), may hold values from -0.125 to 0.125
- norm_gain: float32 [2048], P('tp'), may hold values from 0.1 to 1.9
- up_weight: bfloat16 [2048, 8192], P('sp', 'tp'), may hold values from -0.125 to 0.125
- down_weight: bfloat16 [8192, 2048], P('tp', 'sp'), may hold values from -0.0625 to 0.0625
Outputs:
- layer_out: bfloat16 [2048, 2048], P('sp', 'tp')
All inputs are finite; a program needn't handle non-finite values.
Results may differ from a plain program's by a relative error of at most 0.012.
Values may be sent and summed in bfloat16 or wider, within the bound.
No kernel may reach another device: no remote copies, remote signals or barrier semaphores. Data moves between devices by JAX's collectives and lax.ppermute only.
A program may use at most 128 MiB of HBM per device.

v0:
```python
import jax
import jax.numpy as jnp
from jax import lax
from jax.sharding import PartitionSpec as P

D = 2048
HEADS = 8
KV_HEADS = 2
HEAD_DIM = 128
VALUE_DIM = 256
epsilon = 1e-06


def head_norm(per_map, lambdas, gain):
    difference = per_map[:, 0] - lambdas[:, None, None] * per_map[:, 1]
    scaled = (
        difference
        * lax.rsqrt(jnp.mean(difference * difference, axis=-1, keepdims=True) + epsilon)
        * gain
    )
    return scaled.astype(jnp.bfloat16)


def on_device(
    residual,
    queries,
    key_proj,
    value_proj,
    diff_lambda,
    head_gain,
    out_weight,
    norm_gain,
    up_weight,
    down_weight,
):
    rows_here = residual.shape[0]
    per_group = HEADS // KV_HEADS
    scaling = HEAD_DIM ** (-0.5)
    all_queries = lax.all_gather(queries, "tp", axis=1, tiled=True)
    query_grid = all_queries.reshape(rows_here, KV_HEADS, per_group, 2, HEAD_DIM)
    stat_shape = (KV_HEADS, per_group, 2, rows_here)
    maxima = jnp.full(stat_shape, -1e30, jnp.float32)
    key_piece = lax.all_gather(key_proj, "sp", axis=0, tiled=True)
    value_piece = lax.all_gather(value_proj, "sp", axis=0, tiled=True)
    key_count = key_piece.shape[0]
    key_grid = key_piece.reshape(key_count, KV_HEADS, 2, HEAD_DIM)
    value_grid = value_piece.reshape(key_count, KV_HEADS, VALUE_DIM)
    scores = (
        jnp.einsum("qagcd,kacd->agcqk", query_grid, key_grid, preferred_element_type=jnp.float32)
        * scaling
    )
    highest = jnp.maximum(maxima, jnp.max(scores, axis=-1))
    weights = jnp.exp(scores - highest[..., None])
    totals = jnp.sum(weights, axis=-1)
    weighted = jnp.einsum(
        "agcqk,kae->agcqe",
        weights.astype(jnp.bfloat16),
        value_grid,
        preferred_element_type=jnp.float32,
    )
    maxima, totals, weighted = (highest, totals, weighted)
    maxima = maxima.reshape(HEADS, 2, rows_here)
    totals = totals.reshape(HEADS, 2, rows_here)
    weighted = weighted.reshape(HEADS, 2, rows_here, VALUE_DIM)
    tp_size = lax.axis_size("tp")
    local_heads = HEADS // tp_size
    got_max, got_tot, got_sum = (
        lax.all_to_all(maxima, "tp", split_axis=0, concat_axis=0, tiled=True),
        lax.all_to_all(totals, "tp", split_axis=0, concat_axis=0, tiled=True),
        lax.all_to_all(weighted, "tp", split_axis=0, concat_axis=0, tiled=True),
    )
    got_max = got_max.reshape(tp_size, local_heads, 2, rows_here)
    got_tot = got_tot.reshape(tp_size, local_heads, 2, rows_here)
    got_sum = got_sum.reshape(tp_size, local_heads, 2, rows_here, VALUE_DIM)
    highest = jnp.max(got_max, axis=0)
    factor = jnp.exp(got_max - highest)
    totals_all = jnp.sum(factor * got_tot, axis=0)
    sums_all = jnp.sum(factor[..., None] * got_sum, axis=0)
    lambdas = lax.dynamic_slice_in_dim(diff_lambda, lax.axis_index("tp") * local_heads, local_heads)
    own_heads = head_norm(sums_all / totals_all[..., None], lambdas, head_gain)
    head_outputs = lax.all_gather(own_heads, "tp", axis=0, tiled=True)
    out_grid = out_weight.reshape(HEADS, VALUE_DIM, out_weight.shape[1])
    projected = jnp.einsum(
        "hqe,hed->qd", head_outputs, out_grid, preferred_element_type=jnp.float32
    )
    after_mix = residual.astype(jnp.float32) + projected
    squares = lax.psum(jnp.sum(after_mix * after_mix, axis=1), "tp")
    normed = (after_mix * lax.rsqrt(squares / D + epsilon)[:, None] * norm_gain).astype(
        jnp.bfloat16
    )
    full_rows = lax.all_gather(normed, "tp", axis=1, tiled=True)
    hidden = jnp.dot(
        full_rows,
        lax.all_gather(up_weight, "sp", axis=0, tiled=True),
        preferred_element_type=jnp.float32,
    )
    activated = jnp.square(jax.nn.relu(hidden)).astype(jnp.bfloat16)
    partial_value = jnp.dot(
        activated,
        lax.all_gather(down_weight, "sp", axis=1, tiled=True),
        preferred_element_type=jnp.float32,
    )
    mixer_sum = lax.psum_scatter(partial_value, "tp", scatter_dimension=1, tiled=True)
    return (after_mix + mixer_sum).astype(jnp.bfloat16)


def solution(mesh):
    return jax.shard_map(
        on_device,
        mesh=mesh,
        in_specs=(
            P("sp", "tp"),
            P("sp", "tp"),
            P(("sp", "tp"), None),
            P(("sp", "tp"), None),
            P(),
            P(),
            P(None, "tp"),
            P("tp"),
            P("sp", "tp"),
            P("tp", "sp"),
        ),
        out_specs=P("sp", "tp"),
        check_vma=False,
    )
```

profile of v0, /device:TPU:0, one launch (start us, length us, event | category | flops | bytes accessed | tf_op | source)
XLA Modules:
  0.0 390.0 jit_solution(11635504555220988634)
XLA Ops:
  6.5 0.7 all-gather.5.cloned.1.call-update
  7.3 0.7 all-gather.7.cloned.1.call-update
  8.1 0.7 all-gather.11.cloned.1.call-update
  8.8 0.5 all-gather.9.cloned.1.call-update
  9.3 1.1 copy.32
  10.4 9.9 %all_gather.22 = bf16[128,2048]{0,1:T(8,128)(2,1)S(1)} all-gather(bf16[128,1024]{0,1:T(8,128)(2,1)S(1)} %copy.32), channel_id=1, replica_groups=mesh['sp'=16,'tp'=2] {'tp'}, dimensions={1}, use_global_device_ids=true | all-gather | bytes 786432 | tf_op jit(solution)/shard_map/all_gather | solution.py:39
  20.4 29.7 %all-gather.5.cloned.1.call-done = bf16[1024,512]{1,0:T(8,128)(2,1)} async-done(((bf16[64,512]{1,0:T(8,128)(2,1)}), bf16[1024,512]{1,0:T(8,128)(2,1)}) %all-gather.5.cloned.1.call-update) | async-done | bytes 1048592 | tf_op jit(solution)/shard_map/all_gather | solution.py:43
  50.1 1.5 copy.31
  51.6 4.5 %bitcast_reduce_fusion = (f32[2,4,2,128]{3,1,2,0:T(4,128)S(1)}, f32[2,2,1024,128,4]{3,2,4,1,0:T(8,128)}) fusion(bf16[1024,2,2,128,1]{0,3,4,2,1:T(8,128)(2,1)S(1)} %bitcast.61, bf16[128,2,4,2,128]{0,4,3,2,1:T(8,128)(2,1)S(1)} %bitcast.62), kind=kOutput, calls=%fused_computation.1 | convolution fusion | flops 541063168 | bytes 9969664 | tf_op jit(solution)/shard_map/qagcd,kacd->agcqk/dot_general | solution.py:49
  56.1 0.6 copy.36
  56.7 3.2 all-to-all-start
  60.0 5.6 %fusion.1 = (f32[2,4,2,128]{3,1,2,0:T(4,128)S(1)}, bf16[2,4,2,128,1024]{3,4,1,2,0:T(8,128)(2,1)}) fusion(f32[2,2,1024,128,4]{3,2,4,1,0:T(8,128)} %get-tuple-element.8, f32[2,4,2,128]{3,1,2,0:T(4,128)S(1)} %broadcast_maximum_fusion), kind=kLoop, calls=%fused_computation.3 | loop fusion | flops 8386560 | bytes 12599296 | tf_op jit(solution)/shard_map/reduce_sum | solution.py:54
  65.6 0.6 copy.41
  66.2 23.0 %all-gather.7.cloned.1.call-done = bf16[1024,512]{1,0:T(8,128)(2,1)} async-done(((bf16[64,512]{1,0:T(8,128)(2,1)}), bf16[1024,512]{1,0:T(8,128)(2,1)}) %all-gather.7.cloned.1.call-update) | async-done | bytes 1048592 | tf_op jit(solution)/shard_map/all_gather | solution.py:44
  89.1 1.5 copy.37
  90.6 3.2 all-to-all-start.2
  93.9 5.2 %fusion.5 = f32[2,4,2,128,256]{4,3,2,1,0:T(8,128)} fusion(bf16[1024,2,256,1,1]{0,2,4,3,1:T(8,128)(2,1)S(1)} %bitcast.64, bf16[2,4,2,128,1024]{3,4,1,2,0:T(8,128)(2,1)} %get-tuple-element.6), kind=kOutput, calls=%fused_computation.8 | convolution fusion | flops 1073741824 | bytes 7340032 | tf_op jit(solution)/shard_map/agcqk,kae->agcqe/dot_general | solution.py:55
  99.1 3.8 all-to-all-start.1
  103.2 25.3 %all-to-all-done.1 = f32[8,2,128,256]{3,2,1,0:T(8,128)S(1)} async-done(((f32[8,2,128,256]{3,2,1,0:T(8,128)}), f32[8,2,128,256]{3,2,1,0:T(8,128)S(1)}, u32[]{:S(2)}, u32[]{:S(2)}) %all-to-all-start.1) | async-done | bytes 2097184 | tf_op jit(solution)/shard_map/all_to_all | solution.py:70
  128.4 0.3 multiply_reduce_fusion
  128.8 0.2 broadcast_divide_fusion
  129.0 0.2 multiply_reduce_fusion.2
  129.2 0.1 multiply_convert_fusion.1
  129.4 8.5 %all_gather.24 = bf16[8,128,256]{2,1,0:T(8,128)(2,1)S(1)} all-gather(bf16[4,128,256]{2,1,0:T(8,128)(2,1)S(1)} %multiply_convert_fusion.1), channel_id=1, replica_groups=mesh['sp'=16,'tp'=2] {'tp'}, dimensions={0}, use_global_device_ids=true | all-gather | bytes 786432 | tf_op jit(solution)/shard_map/all_gather | solution.py:81
  137.9 0.8 multiply_reduce_fusion.1
  138.7 4.9 %psum.7 = f32[128]{0:T(128)S(1)} all-reduce(f32[128]{0:T(128)S(1)} %get-tuple-element.9), channel_id=1, replica_groups=mesh['sp'=16,'tp'=2] {'tp'}, use_global_device_ids=true, to_apply=%region_7.0 | all-reduce | flops 128 | bytes 1024 | tf_op jit(solution)/shard_map/psum | solution.py:87
  143.8 7.0 %all_gather.25 = bf16[128,2048]{1,0:T(8,128)(2,1)S(1)} all-gather(bf16[128,1024]{1,0:T(8,128)(2,1)S(1)} %multiply_convert_fusion), channel_id=1, replica_groups=mesh['sp'=16,'tp'=2] {'tp'}, dimensions={1}, use_global_device_ids=true | all-gather | bytes 786432 | tf_op jit(solution)/shard_map/all_gather | solution.py:91
  150.8 69.3 %all-gather.11.cloned.1.call-done = bf16[4096,2048]{1,0:T(8,128)(2,1)} async-done(((bf16[4096,128]{1,0:T(8,128)(2,1)}), bf16[4096,2048]{1,0:T(8,128)(2,1)}) %all-gather.11.cloned.1.call-update) | async-done | bytes 16777232 | tf_op jit(solution)/shard_map/all_gather | solution.py:100
  220.1 126.7 %all-gather.9.cloned.1.call-done = bf16[2048,4096]{1,0:T(8,128)(2,1)} async-done(((bf16[128,4096]{1,0:T(8,128)(2,1)}), bf16[2048,4096]{1,0:T(8,128)(2,1)}) %all-gather.9.cloned.1.call-update) | async-done | bytes 16777232 | tf_op jit(solution)/shard_map/all_gather | solution.py:94
  346.9 16.1 %fusion.8 = f32[128,2048]{1,0:T(8,128)} fusion(bf16[4096,2048]{1,0:T(8,128)(2,1)} %all-gather.11.cloned.1.call-done, bf16[128,2048]{1,0:T(8,128)(2,1)S(1)} %all_gather.25, bf16[2048,4096]{1,0:T(8,128)(2,1)} %all-gather.9.cloned.1.call-done), kind=kOutput, calls=%fused_computation.13 | convolution fusion | flops 4296540160 | bytes 35127296 | tf_op jit(solution)/shard_map/dot_general | solution.py:98
  362.9 18.7 %reduce-scatter.2.cloned.1.call-done = f32[128,1024]{1,0:T(8,128)} async-done(((f32[128,2048]{1,0:T(8,128)}), f32[128,1024]{1,0:T(8,128)}) %reduce-scatter.2.cloned.1.call-update) | async-done | bytes 524304 | tf_op jit(solution)/shard_map/reduce_scatter | solution.py:103
  381.7 1.8 add_convert_fusion
  (28 shorter events, 0.5 us)
Async XLA Ops:
  6.5 43.6 %all-gather.5.cloned.1.call-start = ((), (), s32[]{:S(2)}) async-start(), calls=%async_computation.4 | async-start | bytes 1114112 | tf_op jit(solution)/shard_map/all_gather | solution.py:43
  7.3 81.9 %all-gather.7.cloned.1.call-start = ((), (), s32[]{:S(2)}) async-start(), calls=%async_computation.5 | async-start | bytes 1114112 | tf_op jit(solution)/shard_map/all_gather | solution.py:44
  8.0 212.1 %all-gather.11.cloned.1.call-start = ((), (), s32[]{:S(2)}) async-start(), calls=%async_computation.7 | async-start | bytes 17825792 | tf_op jit(solution)/shard_map/all_gather | solution.py:100
  8.7 338.1 %all-gather.9.cloned.1.call-start = ((), (), s32[]{:S(2)}) async-start(), calls=%async_computation.6 | async-start | bytes 17825792 | tf_op jit(solution)/shard_map/all_gather | solution.py:94
  56.7 33.9 %all-to-all-start = ((f32[8,2,128]{2,1,0:T(2,128)}), f32[8,2,128]{2,1,0:T(2,128)S(1)}, u32[]{:S(2)}, u32[]{:S(2)}) async-start(f32[8,2,128]{2,1,0:T(2,128)} %copy.36), calls=%async_computation | async-start | bytes 16384 | tf_op jit(solution)/shard_map/all_to_all | solution.py:68
  90.6 8.5 %all-to-all-start.2 = ((f32[8,2,128]{2,1,0:T(2,128)}), f32[8,2,128]{2,1,0:T(2,128)S(1)}, u32[]{:S(2)}, u32[]{:S(2)}) async-start(f32[8,2,128]{2,1,0:T(2,128)} %copy.41), calls=%async_computation.2 | async-start | bytes 16384 | tf_op jit(solution)/shard_map/all_to_all | solution.py:69
  93.9 9.1 %copy-start.4 = (f32[8]{0:T(128)S(1)}, f32[8]{0:T(128)}, u32[]{:S(2)}) copy-start(f32[8]{0:T(128)} %param.14) | copy-start | bytes 100
  99.1 29.3 %all-to-all-start.1 = ((f32[8,2,128,256]{3,2,1,0:T(8,128)}), f32[8,2,128,256]{3,2,1,0:T(8,128)S(1)}, u32[]{:S(2)}, u32[]{:S(2)}) async-start(f32[8,2,128,256]{3,2,1,0:T(8,128)} %bitcast.63), calls=%async_computation.1 | async-start | bytes 4194304 | tf_op jit(solution)/shard_map/all_to_all | solution.py:70
  102.9 26.3 %copy-start.3 = (f32[256]{0:T(256)S(1)}, f32[256]{0:T(256)}, u32[]{:S(2)}) copy-start(f32[256]{0:T(256)} %param.15) | copy-start | bytes 3076
  103.0 278.7 %reduce-scatter.2.cloned.1.call-start = ((), (), s32[]{:S(2)}) async-start(), calls=%async_computation.8 | async-start | bytes 1572864 | tf_op jit(solution)/shard_map/reduce_scatter | solution.py:103
  128.4 9.4 %copy-start = (bf16[2048,1024]{1,0:T(8,128)(2,1)S(1)}, bf16[2048,1024]{1,0:T(8,128)(2,1)}, u32[]{:S(2)}) copy-start(bf16[2048,1024]{1,0:T(8,128)(2,1)} %param.16) | copy-start | bytes 12582916
  128.4 9.4 %copy-start.1 = (bf16[128,1024]{1,0:T(8,128)(2,1)S(1)}, bf16[128,1024]{1,0:T(8,128)(2,1)}, u32[]{:S(2)}) copy-start(bf16[128,1024]{1,0:T(8,128)(2,1)} %param.10) | copy-start | bytes 786436
  129.0 14.7 %copy-start.2 = (f32[1024]{0:T(1024)S(1)}, f32[1024]{0:T(1024)}, u32[]{:S(2)}) copy-start(f32[1024]{0:T(1024)} %param.17) | copy-start | bytes 12292
Sparse Core Ops, SparseCore 0:
  9.5 40.5 all-gather.4
  52.3 36.8 all-gather.6
  91.3 128.7 all-gather.10
  222.2 124.6 all-gather.8
  363.1 18.5 reduce-scatter.1
where the time goes:
time: 390 us
  waiting for transfers between devices  295 us (76%)
  blocking collectives  30.4 us (8%)
  matrix products  26.6 us (7%)
  between operations  13.3 us (3%)
  starting transfers between devices  10.4 us (3%)
  other arithmetic  8.51 us (2%)
  local copies, waits for them, and re-layouts  5.4 us (1%)
    all_gather x1, waiting for transfers between devices, on_device(): lax.all_gather(up_weight, 'sp', axis=0, tiled=True)  127 us
    all_gather x1, waiting for transfers between devices, on_device(): lax.all_gather(down_weight, 'sp', axis=1, tiled=True)  69.3 us
    all_gather x1, waiting for transfers between devices, on_device(): key_piece = lax.all_gather(key_proj, 'sp', axis=0, tiled=True)  29.7 us
    all_to_all x1, waiting for transfers between devices, on_device(): lax.all_to_all(weighted, 'tp', split_axis=0, concat_axis=0, tiled=True)  25.3 us
    all_gather x1, waiting for transfers between devices, on_device(): value_piece = lax.all_gather(value_proj, 'sp', axis=0, tiled=True)  23 us
    reduce_scatter x1, waiting for transfers between devices, on_device(): lax.psum_scatter(partial_value, 'tp', scatter_dimension=1, tiled=True)  18.7 us
    dot_general x1, matrix products, on_device(): jnp.dot(activated, lax.all_gather(down_weight, 'sp', axis=1, tiled=True),...  16.1 us
    all_gather x1, blocking collectives, on_device(): all_queries = lax.all_gather(queries, 'tp', axis=1, tiled=True)  9.94 us
  transfers between devices with their start and end apart: 8, of which 6 were waited for; matrix products, arithmetic and copies ran while one was open for 6% of the time, Pallas kernels for 0%

commit v1 on v0

--- a/solution.py
+++ b/solution.py
@@ -40,7 +40,12 @@
     query_grid = all_queries.reshape(rows_here, KV_HEADS, per_group, 2, HEAD_DIM)
     stat_shape = (KV_HEADS, per_group, 2, rows_here)
     maxima = jnp.full(stat_shape, -1e30, jnp.float32)
-    key_piece = lax.all_gather(key_proj, "sp", axis=0, tiled=True)
+    ring = [key_proj]
+    for hop in range(15):
+        ring.append(lax.ppermute(ring[-1], "sp", [(dev, (dev + 1) % 16) for dev in range(16)]))
+    key_piece = jnp.roll(
+        jnp.concatenate(ring[::-1], axis=0), (lax.axis_index("sp") + 1) * ring[0].shape[0], axis=0
+    )
     value_piece = lax.all_gather(value_proj, "sp", axis=0, tiled=True)
     key_count = key_piece.shape[0]
     key_grid = key_piece.reshape(key_count, KV_HEADS, 2, HEAD_DIM)

time: 390 us -> 361 us (0.926)
  waiting for transfers between devices: 295 us -> 261 us
  local copies, waits for them, and re-layouts: 5.4 us -> 11.7 us
    all_gather x1, waiting for transfers between devices: 127 us -> 0.01 us  [on_device(): lax.all_gather(up_weight, 'sp', axis=0, tiled=True)]
    ppermute x0 -> x15, waiting for transfers between devices: none -> 121 us  [on_device(): lax.ppermute(ring[-1], 'sp', [(dev, (dev + 1) % 16) for dev in range(16)])]
    all_gather x1, waiting for transfers between devices: 69.3 us -> 100 us  [on_device(): lax.all_gather(down_weight, 'sp', axis=1, tiled=True)]
    all_gather x1 -> x0, waiting for transfers between devices: 29.7 us -> none  [on_device(): key_piece = lax.all_gather(key_proj, 'sp', axis=0, tiled=True)]
    all_gather x1, waiting for transfers between devices: 23 us -> 0.01 us  [on_device(): value_piece = lax.all_gather(value_proj, 'sp', axis=0, tiled=True)]
    all_to_all x1, waiting for transfers between devices: 25.3 us -> 19 us  [on_device(): lax.all_to_all(weighted, 'tp', split_axis=0, concat_axis=0, tiled=True)]
    concatenate x0 -> x1, local copies, waits for them, and re-layouts: none -> 5.78 us  [on_device(): jnp.roll(jnp.concatenate(ring[::-1], axis=0), (lax.axis_index('sp') + 1)...]
  transfers between devices with their start and end apart: 8 -> 22, of which waited for: 6 -> 18; matrix products, arithmetic and copies ran while one was open for 6% -> 8% of each run, Pallas kernels for 0% -> 0%
where the time goes in v1:
time: 361 us
  waiting for transfers between devices  261 us (72%)
  blocking collectives  28.6 us (8%)
  matrix products  26.7 us (7%)
  between operations  13.4 us (4%)
  local copies, waits for them, and re-layouts  11.7 us (3%)
  starting transfers between devices  11 us (3%)
  other arithmetic  8.54 us (2%)
    ppermute x15, waiting for transfers between devices, on_device(): lax.ppermute(ring[-1], 'sp', [(dev, (dev + 1) % 16) for dev in range(16)])  121 us
    all_gather x1, waiting for transfers between devices, on_device(): lax.all_gather(down_weight, 'sp', axis=1, tiled=True)  100 us
    all_to_all x1, waiting for transfers between devices, on_device(): lax.all_to_all(weighted, 'tp', split_axis=0, concat_axis=0, tiled=True)  19 us
    reduce_scatter x1, waiting for transfers between devices, on_device(): lax.psum_scatter(partial_value, 'tp', scatter_dimension=1, tiled=True)  18.7 us
    dot_general x1, matrix products, on_device(): jnp.dot(activated, lax.all_gather(down_weight, 'sp', axis=1, tiled=True),...  16.1 us
    all_gather x1, blocking collectives, on_device(): head_outputs = lax.all_gather(own_heads, 'tp', axis=0, tiled=True)  9.47 us
    all_gather x1, blocking collectives, on_device(): full_rows = lax.all_gather(normed, 'tp', axis=1, tiled=True)  7.22 us
  transfers between devices with their start and end apart: 22, of which 18 were waited for; matrix products, arithmetic and copies ran while one was open for 8% of the time, Pallas kernels for 0%

profile of v1, /device:TPU:0, one launch (start us, length us, event | category | flops | bytes accessed | tf_op | source)
XLA Modules:
  0.0 360.6 jit_solution(1215682871849931037)
XLA Ops:
  10.2 7.6 %collective-permute-done = bf16[64,512]{0,1:T(8,128)(2,1)S(1)} collective-permute-done((bf16[64,512]{0,1:T(8,128)(2,1)S(1)}, bf16[64,512]{0,1:T(8,128)(2,1)S(1)}, u32[]{:S(2)}, u32[]{:S(2)}) %collective-permute-start) | collective-permute-done | bytes 65568 | tf_op jit(solution)/shard_map/ppermute | solution.py:45
  17.9 7.2 %collective-permute-done.1 = bf16[64,512]{0,1:T(8,128)(2,1)S(1)} collective-permute-done((bf16[64,512]{0,1:T(8,128)(2,1)S(1)}, bf16[64,512]{0,1:T(8,128)(2,1)S(1)}, u32[]{:S(2)}, u32[]{:S(2)}) %collective-permute-start.1) | collective-permute-done | bytes 65568 | tf_op jit(solution)/shard_map/ppermute | solution.py:45
  25.1 7.4 %collective-permute-done.2 = bf16[64,512]{0,1:T(8,128)(2,1)S(1)} collective-permute-done((bf16[64,512]{0,1:T(8,128)(2,1)S(1)}, bf16[64,512]{0,1:T(8,128)(2,1)S(1)}, u32[]{:S(2)}, u32[]{:S(2)}) %collective-permute-start.2) | collective-permute-done | bytes 65568 | tf_op jit(solution)/shard_map/ppermute | solution.py:45
  32.5 7.2 %collective-permute-done.3 = bf16[64,512]{0,1:T(8,128)(2,1)S(1)} collective-permute-done((bf16[64,512]{0,1:T(8,128)(2,1)S(1)}, bf16[64,512]{0,1:T(8,128)(2,1)S(1)}, u32[]{:S(2)}, u32[]{:S(2)}) %collective-permute-start.3) | collective-permute-done | bytes 65568 | tf_op jit(solution)/shard_map/ppermute | solution.py:45
  39.7 8.4 %collective-permute-done.4 = bf16[64,512]{0,1:T(8,128)(2,1)S(1)} collective-permute-done((bf16[64,512]{0,1:T(8,128)(2,1)S(1)}, bf16[64,512]{0,1:T(8,128)(2,1)S(1)}, u32[]{:S(2)}, u32[]{:S(2)}) %collective-permute-start.4) | collective-permute-done | bytes 65568 | tf_op jit(solution)/shard_map/ppermute | solution.py:45
  48.1 7.1 %collective-permute-done.5 = bf16[64,512]{0,1:T(8,128)(2,1)S(1)} collective-permute-done((bf16[64,512]{0,1:T(8,128)(2,1)S(1)}, bf16[64,512]{0,1:T(8,128)(2,1)S(1)}, u32[]{:S(2)}, u32[]{:S(2)}) %collective-permute-start.5) | collective-permute-done | bytes 65568 | tf_op jit(solution)/shard_map/ppermute | solution.py:45
  55.2 7.1 %collective-permute-done.6 = bf16[64,512]{0,1:T(8,128)(2,1)S(1)} collective-permute-done((bf16[64,512]{0,1:T(8,128)(2,1)S(1)}, bf16[64,512]{0,1:T(8,128)(2,1)S(1)}, u32[]{:S(2)}, u32[]{:S(2)}) %collective-permute-start.6) | collective-permute-done | bytes 65568 | tf_op jit(solution)/shard_map/ppermute | solution.py:45
  62.3 9.9 %collective-permute-done.7 = bf16[64,512]{0,1:T(8,128)(2,1)S(1)} collective-permute-done((bf16[64,512]{0,1:T(8,128)(2,1)S(1)}, bf16[64,512]{0,1:T(8,128)(2,1)S(1)}, u32[]{:S(2)}, u32[]{:S(2)}) %collective-permute-start.7) | collective-permute-done | bytes 65568 | tf_op jit(solution)/shard_map/ppermute | solution.py:45
  72.2 10.0 %collective-permute-done.8 = bf16[64,512]{0,1:T(8,128)(2,1)S(1)} collective-permute-done((bf16[64,512]{0,1:T(8,128)(2,1)S(1)}, bf16[64,512]{0,1:T(8,128)(2,1)S(1)}, u32[]{:S(2)}, u32[]{:S(2)}) %collective-permute-start.8) | collective-permute-done | bytes 65568 | tf_op jit(solution)/shard_map/ppermute | solution.py:45
  82.2 10.0 %collective-permute-done.9 = bf16[64,512]{0,1:T(8,128)(2,1)S(1)} collective-permute-done((bf16[64,512]{0,1:T(8,128)(2,1)S(1)}, bf16[64,512]{0,1:T(8,128)(2,1)S(1)}, u32[]{:S(2)}, u32[]{:S(2)}) %collective-permute-start.9) | collective-permute-done | bytes 65568 | tf_op jit(solution)/shard_map/ppermute | solution.py:45
  92.2 10.0 %collective-permute-done.10 = bf16[64,512]{0,1:T(8,128)(2,1)S(1)} collective-permute-done((bf16[64,512]{0,1:T(8,128)(2,1)S(1)}, bf16[64,512]{0,1:T(8,128)(2,1)S(1)}, u32[]{:S(2)}, u32[]{:S(2)}) %collective-permute-start.10) | collective-permute-done | bytes 65568 | tf_op jit(solution)/shard_map/ppermute | solution.py:45
  102.3 7.1 %collective-permute-done.11 = bf16[64,512]{0,1:T(8,128)(2,1)S(1)} collective-permute-done((bf16[64,512]{0,1:T(8,128)(2,1)S(1)}, bf16[64,512]{0,1:T(8,128)(2,1)S(1)}, u32[]{:S(2)}, u32[]{:S(2)}) %collective-permute-start.11) | collective-permute-done | bytes 65568 | tf_op jit(solution)/shard_map/ppermute | solution.py:45
  109.3 9.9 %collective-permute-done.12 = bf16[64,512]{0,1:T(8,128)(2,1)S(1)} collective-permute-done((bf16[64,512]{0,1:T(8,128)(2,1)S(1)}, bf16[64,512]{0,1:T(8,128)(2,1)S(1)}, u32[]{:S(2)}, u32[]{:S(2)}) %collective-permute-start.12) | collective-permute-done | bytes 65568 | tf_op jit(solution)/shard_map/ppermute | solution.py:45
  120.5 8.9 %collective-permute-done.13 = bf16[64,512]{0,1:T(8,128)(2,1)S(1)} collective-permute-done((bf16[64,512]{0,1:T(8,128)(2,1)S(1)}, bf16[64,512]{0,1:T(8,128)(2,1)S(1)}, u32[]{:S(2)}, u32[]{:S(2)}) %collective-permute-start.13) | collective-permute-done | bytes 65568 | tf_op jit(solution)/shard_map/ppermute | solution.py:45
  129.4 7.0 %all_gather.18 = bf16[128,2048]{0,1:T(8,128)(2,1)S(1)} all-gather(bf16[128,1024]{0,1:T(8,128)(2,1)S(1)} %copy.38), channel_id=1, replica_groups=mesh['sp'=16,'tp'=2] {'tp'}, dimensions={1}, use_global_device_ids=true | all-gather | bytes 786432 | tf_op jit(solution)/shard_map/all_gather | solution.py:39
  136.4 3.1 collective-permute-done.14
  139.5 5.8 %concatenate.6 = bf16[2048,512]{0,1:T(8,128)(2,1)S(1)} concatenate(bf16[64,512]{0,1:T(8,128)(2,1)} %collective-permute-done.14, bf16[64,512]{0,1:T(8,128)(2,1)} %copy-done.8, bf16[64,512]{0,1:T(8,128)(2,1)} %copy-done.7, bf16[64,512]{0,1:T(8,128)(2,1)} %copy-done.6, bf16[64,512]{0,1:T(8,128)(2,1)} %copy-done.5, bf16[64,512]{0,1:T(8,128)(2,1)} %copy-done.4, ...), dimensions={0} | concatenate | bytes 4194304 | tf_op jit(solution)/shard_map/jit(_roll_dynamic)/concatenate | solution.py:46
  146.0 4.5 %bitcast_reduce_fusion = (f32[2,4,2,128]{3,1,2,0:T(4,128)S(1)}, f32[2,2,1024,128,4]{3,2,4,1,0:T(8,128)}) fusion(bf16[1024,2,2,128,1]{0,3,4,2,1:T(8,128)(2,1)S(1)} %bitcast.61, bf16[128,2,4,2,128]{0,4,3,2,1:T(8,128)(2,1)S(1)} %bitcast.62), kind=kOutput, calls=%fused_computation.1 | convolution fusion | flops 541063168 | bytes 9969664 | tf_op jit(solution)/shard_map/qagcd,kacd->agcqk/dot_general | solution.py:54
  151.2 3.2 all-to-all-start
  154.4 5.7 %fusion.1 = (f32[2,4,2,128]{3,1,2,0:T(4,128)S(1)}, bf16[2,4,2,128,1024]{3,4,1,2,0:T(8,128)(2,1)}) fusion(f32[2,2,1024,128,4]{3,2,4,1,0:T(8,128)} %get-tuple-element.8, f32[2,4,2,128]{3,1,2,0:T(4,128)S(1)} %broadcast_maximum_fusion), kind=kLoop, calls=%fused_computation.3 | loop fusion | flops 8386560 | bytes 12599296 | tf_op jit(solution)/shard_map/reduce_sum | solution.py:59
  160.7 1.7 copy.43
  162.4 3.2 all-to-all-start.2
  165.7 5.2 %fusion.5 = f32[2,4,2,128,256]{4,3,2,1,0:T(8,128)} fusion(bf16[1024,2,256,1,1]{0,2,4,3,1:T(8,128)(2,1)S(1)} %bitcast.64, bf16[2,4,2,128,1024]{3,4,1,2,0:T(8,128)(2,1)} %get-tuple-element.6), kind=kOutput, calls=%fused_computation.8 | convolution fusion | flops 1073741824 | bytes 7340032 | tf_op jit(solution)/shard_map/agcqk,kae->agcqe/dot_general | solution.py:60
  170.9 3.8 %all-to-all-start.1 = ((f32[8,2,128,256]{3,2,1,0:T(8,128)}), f32[8,2,128,256]{3,2,1,0:T(8,128)S(1)}, u32[]{:S(2)}, u32[]{:S(2)}) async-start(f32[8,2,128,256]{3,2,1,0:T(8,128)} %bitcast.63), calls=%async_computation.1 | async-start | bytes 4194304 | tf_op jit(solution)/shard_map/all_to_all | solution.py:75
  174.9 19.0 %all-to-all-done.1 = f32[8,2,128,256]{3,2,1,0:T(8,128)S(1)} async-done(((f32[8,2,128,256]{3,2,1,0:T(8,128)}), f32[8,2,128,256]{3,2,1,0:T(8,128)S(1)}, u32[]{:S(2)}, u32[]{:S(2)}) %all-to-all-start.1) | async-done | bytes 2097184 | tf_op jit(solution)/shard_map/all_to_all | solution.py:75
  194.9 9.5 %all_gather.20 = bf16[8,128,256]{2,1,0:T(8,128)(2,1)S(1)} all-gather(bf16[4,128,256]{2,1,0:T(8,128)(2,1)S(1)} %multiply_convert_fusion.1), channel_id=1, replica_groups=mesh['sp'=16,'tp'=2] {'tp'}, dimensions={0}, use_global_device_ids=true | all-gather | bytes 786432 | tf_op jit(solution)/shard_map/all_gather | solution.py:86
  205.2 4.9 %psum.7 = f32[128]{0:T(128)S(1)} all-reduce(f32[128]{0:T(128)S(1)} %get-tuple-element.9), channel_id=1, replica_groups=mesh['sp'=16,'tp'=2] {'tp'}, use_global_device_ids=true, to_apply=%region_7.8 | all-reduce | flops 128 | bytes 1024 | tf_op jit(solution)/shard_map/psum | solution.py:92
  210.2 7.2 %all_gather.21 = bf16[128,2048]{1,0:T(8,128)(2,1)S(1)} all-gather(bf16[128,1024]{1,0:T(8,128)(2,1)S(1)} %multiply_convert_fusion), channel_id=1, replica_groups=mesh['sp'=16,'tp'=2] {'tp'}, dimensions={1}, use_global_device_ids=true | all-gather | bytes 786432 | tf_op jit(solution)/shard_map/all_gather | solution.py:96
  217.5 100.0 %all-gather.8.cloned.1.call-done = bf16[4096,2048]{1,0:T(8,128)(2,1)} async-done(((bf16[4096,128]{1,0:T(8,128)(2,1)}), bf16[4096,2048]{1,0:T(8,128)(2,1)}) %all-gather.8.cloned.1.call-update) | async-done | bytes 16777232 | tf_op jit(solution)/shard_map/all_gather | solution.py:105
  317.4 16.1 %fusion.8 = f32[128,2048]{1,0:T(8,128)} fusion(bf16[4096,2048]{1,0:T(8,128)(2,1)} %all-gather.8.cloned.1.call-done, bf16[128,2048]{1,0:T(8,128)(2,1)S(1)} %all_gather.21, bf16[2048,4096]{1,0:T(8,128)(2,1)} %all-gather.6.cloned.1.call-done), kind=kOutput, calls=%fused_computation.13 | convolution fusion | flops 4296540160 | bytes 35127296 | tf_op jit(solution)/shard_map/dot_general | solution.py:103
  333.6 18.7 %reduce-scatter.2.cloned.1.call-done = f32[128,1024]{1,0:T(8,128)} async-done(((f32[128,2048]{1,0:T(8,128)}), f32[128,1024]{1,0:T(8,128)}) %reduce-scatter.2.cloned.1.call-update) | async-done | bytes 524304 | tf_op jit(solution)/shard_map/reduce_scatter | solution.py:108
  352.3 1.8 add_convert_fusion
  (73 shorter events, 8.9 us)
Async XLA Ops:
  6.5 154.1 %all-gather.4.cloned.1.call-start = ((), (), s32[]{:S(2)}) async-start(), calls=%async_computation.4 | async-start | bytes 1114112 | tf_op jit(solution)/shard_map/all_gather | solution.py:49
  7.3 210.2 %all-gather.6.cloned.1.call-start = ((), (), s32[]{:S(2)}) async-start(), calls=%async_computation.5 | async-start | bytes 17825792 | tf_op jit(solution)/shard_map/all_gather | solution.py:99
  8.0 309.4 %all-gather.8.cloned.1.call-start = ((), (), s32[]{:S(2)}) async-start(), calls=%async_computation.6 | async-start | bytes 17825792 | tf_op jit(solution)/shard_map/all_gather | solution.py:105
  9.7 8.2 %collective-permute-start = (bf16[64,512]{0,1:T(8,128)(2,1)S(1)}, bf16[64,512]{0,1:T(8,128)(2,1)S(1)}, u32[]{:S(2)}, u32[]{:S(2)}) collective-permute-start(bf16[64,512]{0,1:T(8,128)(2,1)S(1)} %copy.35), channel_id=1, source_target_pairs={{0,2},{2,4},{4,6},{6,8},{8,10},{10,12},{12,14},{14,16},{16,18},{18... | collective-permute-start | bytes 196616 | tf_op jit(solution)/shard_map/ppermute | solution.py:45
  17.9 7.2 %collective-permute-start.1 = (bf16[64,512]{0,1:T(8,128)(2,1)S(1)}, bf16[64,512]{0,1:T(8,128)(2,1)S(1)}, u32[]{:S(2)}, u32[]{:S(2)}) collective-permute-start(bf16[64,512]{0,1:T(8,128)(2,1)S(1)} %collective-permute-done), channel_id=1, source_target_pairs={{0,2},{2,4},{4,6},{6,8},{8,10},{10,12},{12,14},{14,16},{16,18},{18... | collective-permute-start | bytes 196616 | tf_op jit(solution)/shard_map/ppermute | solution.py:45
  25.1 7.4 %collective-permute-start.2 = (bf16[64,512]{0,1:T(8,128)(2,1)S(1)}, bf16[64,512]{0,1:T(8,128)(2,1)S(1)}, u32[]{:S(2)}, u32[]{:S(2)}) collective-permute-start(bf16[64,512]{0,1:T(8,128)(2,1)S(1)} %collective-permute-done.1), channel_id=1, source_target_pairs={{0,2},{2,4},{4,6},{6,8},{8,10},{10,12},{12,14},{14,16},{16,18},{18... | collective-permute-start | bytes 196616 | tf_op jit(solution)/shard_map/ppermute | solution.py:45
  32.5 7.2 %collective-permute-start.3 = (bf16[64,512]{0,1:T(8,128)(2,1)S(1)}, bf16[64,512]{0,1:T(8,128)(2,1)S(1)}, u32[]{:S(2)}, u32[]{:S(2)}) collective-permute-start(bf16[64,512]{0,1:T(8,128)(2,1)S(1)} %collective-permute-done.2), channel_id=1, source_target_pairs={{0,2},{2,4},{4,6},{6,8},{8,10},{10,12},{12,14},{14,16},{16,18},{18... | collective-permute-start | bytes 196616 | tf_op jit(solution)/shard_map/ppermute | solution.py:45
  39.7 8.4 %collective-permute-start.4 = (bf16[64,512]{0,1:T(8,128)(2,1)S(1)}, bf16[64,512]{0,1:T(8,128)(2,1)S(1)}, u32[]{:S(2)}, u32[]{:S(2)}) collective-permute-start(bf16[64,512]{0,1:T(8,128)(2,1)S(1)} %collective-permute-done.3), channel_id=1, source_target_pairs={{0,2},{2,4},{4,6},{6,8},{8,10},{10,12},{12,14},{14,16},{16,18},{18... | collective-permute-start | bytes 196616 | tf_op jit(solution)/shard_map/ppermute | solution.py:45
  48.1 7.1 %collective-permute-start.5 = (bf16[64,512]{0,1:T(8,128)(2,1)S(1)}, bf16[64,512]{0,1:T(8,128)(2,1)S(1)}, u32[]{:S(2)}, u32[]{:S(2)}) collective-permute-start(bf16[64,512]{0,1:T(8,128)(2,1)S(1)} %collective-permute-done.4), channel_id=1, source_target_pairs={{0,2},{2,4},{4,6},{6,8},{8,10},{10,12},{12,14},{14,16},{16,18},{18... | collective-permute-start | bytes 196616 | tf_op jit(solution)/shard_map/ppermute | solution.py:45
  55.2 7.1 %collective-permute-start.6 = (bf16[64,512]{0,1:T(8,128)(2,1)S(1)}, bf16[64,512]{0,1:T(8,128)(2,1)S(1)}, u32[]{:S(2)}, u32[]{:S(2)}) collective-permute-start(bf16[64,512]{0,1:T(8,128)(2,1)S(1)} %collective-permute-done.5), channel_id=1, source_target_pairs={{0,2},{2,4},{4,6},{6,8},{8,10},{10,12},{12,14},{14,16},{16,18},{18... | collective-permute-start | bytes 196616 | tf_op jit(solution)/shard_map/ppermute | solution.py:45
  62.3 57.0 %copy-start.1 = (bf16[64,512]{0,1:T(8,128)(2,1)}, bf16[64,512]{0,1:T(8,128)(2,1)S(1)}, u32[]{:S(2)}) copy-start(bf16[64,512]{0,1:T(8,128)(2,1)S(1)} %collective-permute-done.6) | copy-start | bytes 196612
  62.3 9.9 %collective-permute-start.7 = (bf16[64,512]{0,1:T(8,128)(2,1)S(1)}, bf16[64,512]{0,1:T(8,128)(2,1)S(1)}, u32[]{:S(2)}, u32[]{:S(2)}) collective-permute-start(bf16[64,512]{0,1:T(8,128)(2,1)S(1)} %collective-permute-done.6), channel_id=1, source_target_pairs={{0,2},{2,4},{4,6},{6,8},{8,10},{10,12},{12,14},{14,16},{16,18},{18... | collective-permute-start | bytes 196616 | tf_op jit(solution)/shard_map/ppermute | solution.py:45
  72.2 47.1 %copy-start.2 = (bf16[64,512]{0,1:T(8,128)(2,1)}, bf16[64,512]{0,1:T(8,128)(2,1)S(1)}, u32[]{:S(2)}) copy-start(bf16[64,512]{0,1:T(8,128)(2,1)S(1)} %collective-permute-done.7) | copy-start | bytes 196612
  72.2 10.0 %collective-permute-start.8 = (bf16[64,512]{0,1:T(8,128)(2,1)S(1)}, bf16[64,512]{0,1:T(8,128)(2,1)S(1)}, u32[]{:S(2)}, u32[]{:S(2)}) collective-permute-start(bf16[64,512]{0,1:T(8,128)(2,1)S(1)} %collective-permute-done.7), channel_id=1, source_target_pairs={{0,2},{2,4},{4,6},{6,8},{8,10},{10,12},{12,14},{14,16},{16,18},{18... | collective-permute-start | bytes 196616 | tf_op jit(solution)/shard_map/ppermute | solution.py:45
  82.2 37.0 %copy-start.3 = (bf16[64,512]{0,1:T(8,128)(2,1)}, bf16[64,512]{0,1:T(8,128)(2,1)S(1)}, u32[]{:S(2)}) copy-start(bf16[64,512]{0,1:T(8,128)(2,1)S(1)} %collective-permute-done.8) | copy-start | bytes 196612
  82.2 10.0 %collective-permute-start.9 = (bf16[64,512]{0,1:T(8,128)(2,1)S(1)}, bf16[64,512]{0,1:T(8,128)(2,1)S(1)}, u32[]{:S(2)}, u32[]{:S(2)}) collective-permute-start(bf16[64,512]{0,1:T(8,128)(2,1)S(1)} %collective-permute-done.8), channel_id=1, source_target_pairs={{0,2},{2,4},{4,6},{6,8},{8,10},{10,12},{12,14},{14,16},{16,18},{18... | collective-permute-start | bytes 196616 | tf_op jit(solution)/shard_map/ppermute | solution.py:45
  92.2 27.0 %copy-start.4 = (bf16[64,512]{0,1:T(8,128)(2,1)}, bf16[64,512]{0,1:T(8,128)(2,1)S(1)}, u32[]{:S(2)}) copy-start(bf16[64,512]{0,1:T(8,128)(2,1)S(1)} %collective-permute-done.9) | copy-start | bytes 196612
  92.2 10.0 %collective-permute-start.10 = (bf16[64,512]{0,1:T(8,128)(2,1)S(1)}, bf16[64,512]{0,1:T(8,128)(2,1)S(1)}, u32[]{:S(2)}, u32[]{:S(2)}) collective-permute-start(bf16[64,512]{0,1:T(8,128)(2,1)S(1)} %collective-permute-done.9), channel_id=1, source_target_pairs={{0,2},{2,4},{4,6},{6,8},{8,10},{10,12},{12,14},{14,16},{16,18},{18... | collective-permute-start | bytes 196616 | tf_op jit(solution)/shard_map/ppermute | solution.py:45
  102.2 17.0 %copy-start.5 = (bf16[64,512]{0,1:T(8,128)(2,1)}, bf16[64,512]{0,1:T(8,128)(2,1)S(1)}, u32[]{:S(2)}) copy-start(bf16[64,512]{0,1:T(8,128)(2,1)S(1)} %collective-permute-done.10) | copy-start | bytes 196612
  102.2 7.1 %collective-permute-start.11 = (bf16[64,512]{0,1:T(8,128)(2,1)S(1)}, bf16[64,512]{0,1:T(8,128)(2,1)S(1)}, u32[]{:S(2)}, u32[]{:S(2)}) collective-permute-start(bf16[64,512]{0,1:T(8,128)(2,1)S(1)} %collective-permute-done.10), channel_id=1, source_target_pairs={{0,2},{2,4},{4,6},{6,8},{8,10},{10,12},{12,14},{14,16},{16,18},{18... | collective-permute-start | bytes 196616 | tf_op jit(solution)/shard_map/ppermute | solution.py:45
  109.3 9.9 %collective-permute-start.12 = (bf16[64,512]{0,1:T(8,128)(2,1)S(1)}, bf16[64,512]{0,1:T(8,128)(2,1)S(1)}, u32[]{:S(2)}, u32[]{:S(2)}) collective-permute-start(bf16[64,512]{0,1:T(8,128)(2,1)S(1)} %collective-permute-done.11), channel_id=1, source_target_pairs={{0,2},{2,4},{4,6},{6,8},{8,10},{10,12},{12,14},{14,16},{16,18},{18... | collective-permute-start | bytes 196616 | tf_op jit(solution)/shard_map/ppermute | solution.py:45
  119.3 17.1 %copy-start.7 = (bf16[64,512]{0,1:T(8,128)(2,1)}, bf16[64,512]{0,1:T(8,128)(2,1)S(1)}, u32[]{:S(2)}) copy-start(bf16[64,512]{0,1:T(8,128)(2,1)S(1)} %collective-permute-done.12) | copy-start | bytes 196612
  119.3 10.1 %collective-permute-start.13 = (bf16[64,512]{0,1:T(8,128)(2,1)S(1)}, bf16[64,512]{0,1:T(8,128)(2,1)S(1)}, u32[]{:S(2)}, u32[]{:S(2)}) collective-permute-start(bf16[64,512]{0,1:T(8,128)(2,1)S(1)} %collective-permute-done.12), channel_id=1, source_target_pairs={{0,2},{2,4},{4,6},{6,8},{8,10},{10,12},{12,14},{14,16},{16,18},{18... | collective-permute-start | bytes 196616 | tf_op jit(solution)/shard_map/ppermute | solution.py:45
  129.4 10.1 %collective-permute-start.14 = (bf16[64,512]{0,1:T(8,128)(2,1)S(1)}, bf16[64,512]{0,1:T(8,128)(2,1)}, u32[]{:S(2)}, u32[]{:S(2)}) collective-permute-start(bf16[64,512]{0,1:T(8,128)(2,1)S(1)} %collective-permute-done.13), channel_id=1, source_target_pairs={{0,2},{2,4},{4,6},{6,8},{8,10},{10,12},{12,14},{14,16},{16,18},{18... | collective-permute-start | bytes 196616 | tf_op jit(solution)/shard_map/ppermute | solution.py:45
  151.2 11.3 %all-to-all-start = ((f32[8,2,128]{2,1,0:T(2,128)}), f32[8,2,128]{2,1,0:T(2,128)S(1)}, u32[]{:S(2)}, u32[]{:S(2)}) async-start(f32[8,2,128]{2,1,0:T(2,128)} %copy.42), calls=%async_computation | async-start | bytes 16384 | tf_op jit(solution)/shard_map/all_to_all | solution.py:73
  162.4 8.5 %all-to-all-start.2 = ((f32[8,2,128]{2,1,0:T(2,128)}), f32[8,2,128]{2,1,0:T(2,128)S(1)}, u32[]{:S(2)}, u32[]{:S(2)}) async-start(f32[8,2,128]{2,1,0:T(2,128)} %copy.47), calls=%async_computation.2 | async-start | bytes 16384 | tf_op jit(solution)/shard_map/all_to_all | solution.py:74
  170.9 23.0 %all-to-all-start.1 = ((f32[8,2,128,256]{3,2,1,0:T(8,128)}), f32[8,2,128,256]{3,2,1,0:T(8,128)S(1)}, u32[]{:S(2)}, u32[]{:S(2)}) async-start(f32[8,2,128,256]{3,2,1,0:T(8,128)} %bitcast.63), calls=%async_computation.1 | async-start | bytes 4194304 | tf_op jit(solution)/shard_map/all_to_all | solution.py:75
  174.7 20.0 %copy-start.11 = (f32[256]{0:T(256)S(1)}, f32[256]{0:T(256)}, u32[]{:S(2)}) copy-start(f32[256]{0:T(256)} %param.15) | copy-start | bytes 3076
  174.7 177.6 %reduce-scatter.2.cloned.1.call-start = ((), (), s32[]{:S(2)}) async-start(), calls=%async_computation.7 | async-start | bytes 1572864 | tf_op jit(solution)/shard_map/reduce_scatter | solution.py:108
  193.9 10.4 %copy-start = (bf16[2048,1024]{1,0:T(8,128)(2,1)S(1)}, bf16[2048,1024]{1,0:T(8,128)(2,1)}, u32[]{:S(2)}) copy-start(bf16[2048,1024]{1,0:T(8,128)(2,1)} %param.16) | copy-start | bytes 12582916
  193.9 10.4 %copy-start.9 = (bf16[128,1024]{1,0:T(8,128)(2,1)S(1)}, bf16[128,1024]{1,0:T(8,128)(2,1)}, u32[]{:S(2)}) copy-start(bf16[128,1024]{1,0:T(8,128)(2,1)} %param.10) | copy-start | bytes 786436
  194.5 15.6 %copy-start.10 = (f32[1024]{0:T(1024)S(1)}, f32[1024]{0:T(1024)}, u32[]{:S(2)}) copy-start(f32[1024]{0:T(1024)} %param.17) | copy-start | bytes 12292
  (3 other events, 26.0 us)
Sparse Core Ops, SparseCore 0:
  9.5 41.1 all-gather.3
  52.9 132.6 all-gather.5
  187.8 129.6 all-gather.7
  333.7 18.5 reduce-scatter.1
